TPU v7x, 256 devices: a whole 4x4x8 slice. The times are simulated.
256 devices in a mesh: sp: 16 (over y, x), tp: 16 (over z, core).
Axes of the slice: x: 4, y: 4, z: 8, core: 2. Of those that a mesh axis runs over, the one named last changes fastest.
Arguments:
- conv_value: bfloat16 [49152, 2048], P('sp', 'tp'), may hold values from -48 to 48
- conv_gate: bfloat16 [49152, 2048], P('sp', 'tp'), may hold values from -6 to 6
- doc_ids: int32 [49152], P('sp'), may hold values from 0 to 15, never falling along the last dimension, each value on 1 to 9216 neighbouring positions
- conv_kernel: bfloat16 [31, 2048], P(None, 'tp'), may hold values from -1 to 1
- norm_gain_conv: float32 [2048], replicated, may hold values from 0.1 to 1.9
- norm_bias_conv: float32 [2048], replicated, may hold values from -3 to 3
- proj_weight: bfloat16 [2048, 2048], P('tp'), may hold values from -0.125 to 0.125
- residual: bfloat16 [49152, 2048], P(('sp', 'tp')), may hold values from -6 to 6
- norm_gain_moe: float32 [2048], replicated, may hold values from 0.1 to 1.9
- group_router: bfloat16 [2048, 2], replicated, may hold values from -0.125 to 0.125
- expert_router: bfloat16 [2048, 16], replicated, may hold values from -0.125 to 0.125
- routing: int32 [49152, 2], P(('sp', 'tp')), may hold values from 0 to 15, as said below
- expert_gate_w: bfloat16 [16, 2048, 512], P('sp'), may hold values from -0.125 to 0.125
- expert_up_w: bfloat16 [16, 2048, 512], P('sp'), may hold values from -0.125 to 0.125
- expert_down_w: bfloat16 [16, 512, 2048], P('sp'), may hold values from -0.25 to 0.25
Outputs:
- output: bfloat16 [49152, 2048], P(('sp', 'tp'))
Inputs may be any that keep to these rules, and one draw needn't show every extreme that they name: `routing`: both numbers of a row are different experts of one group (expert // 8); within the rows of one device (aligned blocks of 192 rows) every expert is named exactly 24 times.
All inputs are finite; a program needn't handle non-finite values.
Results may differ from a plain program's by a relative error of at most 0.015.
Values may be sent and summed in bfloat16 or wider, within the bound.
No kernel may reach another device: no remote copies, remote signals or barrier semaphores. Data moves between devices by JAX's collectives and lax.ppermute only.
A program may use at most 64 MiB of HBM per device.

v0:
```python
import jax
import jax.numpy as jnp
from jax import lax
from jax.sharding import PartitionSpec as P

epsilon = 1e-06


def shifted(array, axis, by):
    count = lax.axis_size(axis)
    pairs = [(i, i + by) for i in range(count) if 0 <= i + by < count]
    return lax.ppermute(array, axis, pairs)


def project_rows(activated_rows, proj_weight):
    return jnp.dot(
        activated_rows,
        lax.all_gather(proj_weight, "tp", axis=0, tiled=True),
        preferred_element_type=jnp.float32,
    )


def body(
    conv_value,
    conv_gate,
    doc_ids,
    conv_kernel,
    norm_gain_conv,
    norm_bias_conv,
    proj_weight,
    residual,
    norm_gain_moe,
    group_router,
    expert_router,
    routing,
    expert_gate_w,
    expert_up_w,
    expert_down_w,
):
    local_tokens, local_width = conv_value.shape
    kernel_taps = conv_kernel.shape[0]
    rim_width = kernel_taps - 1
    gated_values = (
        conv_value.astype(jnp.float32) * jax.nn.sigmoid(conv_gate.astype(jnp.float32))
    ).astype(jnp.bfloat16)
    rim_values, rim_ids = shifted(
        (gated_values[local_tokens - rim_width :], doc_ids[local_tokens - rim_width :]), "sp", 1
    )
    padded = jnp.concatenate([rim_values, gated_values], axis=0)
    padded_ids = jnp.concatenate([rim_ids, doc_ids], axis=0)
    kernel = conv_kernel.astype(jnp.float32)
    summed = jnp.zeros((local_tokens, local_width), jnp.float32)
    for tap in range(kernel_taps):
        same_doc = padded_ids[tap : tap + local_tokens] == doc_ids
        summed = summed + jnp.where(
            same_doc[:, None],
            padded[tap : tap + local_tokens].astype(jnp.float32) * kernel[tap][None, :],
            jnp.float32(0.0),
        )
    convolved = summed.astype(jnp.bfloat16)
    raw_rows = lax.all_to_all(convolved, "tp", split_axis=0, concat_axis=1, tiled=True)
    raw_values = raw_rows.astype(jnp.float32)
    average = jnp.mean(raw_values, axis=1, keepdims=True)
    centered = raw_values - average
    variance = jnp.mean(centered * centered, axis=1, keepdims=True)
    moved_rows = jax.nn.silu(
        centered * lax.rsqrt(variance + epsilon) * norm_gain_conv + norm_bias_conv
    ).astype(jnp.bfloat16)
    projected = project_rows(moved_rows, proj_weight)
    state_values = residual.astype(jnp.float32) + projected
    hidden_state = state_values.astype(jnp.bfloat16)
    state_values = hidden_state.astype(jnp.float32)
    normed = (
        state_values
        * lax.rsqrt(jnp.mean(state_values * state_values, axis=1, keepdims=True) + epsilon)
        * norm_gain_moe
    ).astype(jnp.bfloat16)
    group_logits = jnp.dot(normed, group_router, preferred_element_type=jnp.float32)
    expert_logits = jnp.dot(normed, expert_router, preferred_element_type=jnp.float32)
    group_total = group_router.shape[1]
    expert_total = expert_router.shape[1]
    per_group = expert_total // group_total
    first_choice = routing[:, 0]
    second_choice = routing[:, 1]
    chosen_group = first_choice // per_group
    group_exp = jnp.exp(group_logits)
    group_match = chosen_group[:, None] == jnp.arange(group_total, dtype=jnp.int32)[None, :]
    group_prob = jnp.sum(jnp.where(group_match, group_exp, jnp.float32(0.0)), axis=1) / jnp.sum(
        group_exp, axis=1
    )
    expert_iota = jnp.arange(expert_total, dtype=jnp.int32)[None, :]
    first_logit = jnp.sum(
        jnp.where(first_choice[:, None] == expert_iota, expert_logits, jnp.float32(0.0)), axis=1
    )
    second_logit = jnp.sum(
        jnp.where(second_choice[:, None] == expert_iota, expert_logits, jnp.float32(0.0)), axis=1
    )
    first_exp = jnp.exp(first_logit)
    second_exp = jnp.exp(second_logit)
    first_weight = group_prob * first_exp / (first_exp + second_exp)
    second_weight = group_prob * second_exp / (first_exp + second_exp)
    row_count = normed.shape[0]
    capacity = 2 * row_count // expert_total
    flat_experts = routing.reshape(-1)
    indicator = (flat_experts[:, None] == expert_iota).astype(jnp.int32)
    before = jnp.cumsum(indicator, axis=0) - indicator
    position = jnp.sum(before * indicator, axis=1)
    destination = flat_experts * capacity + position
    source = (
        jnp.zeros((2 * row_count,), jnp.int32)
        .at[destination]
        .set(jnp.arange(2 * row_count, dtype=jnp.int32) // 2)
    )
    outgoing = normed[source].reshape(expert_total, capacity, normed.shape[1])
    arrived = lax.all_to_all(outgoing, "sp", split_axis=0, concat_axis=0, tiled=True)
    senders, slot_count, features = arrived.shape
    flattened = arrived.reshape(senders * slot_count, features)
    gate_part = jnp.dot(flattened, expert_gate_w[0], preferred_element_type=jnp.float32)
    up_part = jnp.dot(flattened, expert_up_w[0], preferred_element_type=jnp.float32)
    expert_hidden = (jax.nn.silu(gate_part) * up_part).astype(jnp.bfloat16)
    expert_result = jnp.dot(
        expert_hidden, expert_down_w[0], preferred_element_type=jnp.float32
    ).astype(jnp.bfloat16)
    returned = lax.all_to_all(
        expert_result.reshape(senders, slot_count, features),
        "sp",
        split_axis=0,
        concat_axis=0,
        tiled=True,
    )
    picked = (
        returned.reshape(2 * row_count, normed.shape[1])[destination]
        .reshape(row_count, 2, normed.shape[1])
        .astype(jnp.float32)
    )
    mixture = first_weight[:, None] * picked[:, 0] + second_weight[:, None] * picked[:, 1]
    return (state_values + mixture).astype(jnp.bfloat16)


def solution(mesh):
    placed = (
        P("sp", "tp"),
        P("sp", "tp"),
        P("sp"),
        P(None, "tp"),
        P(),
        P(),
        P("tp", None),
        P(("sp", "tp"), None),
        P(),
        P(),
        P(),
        P(("sp", "tp"), None),
        P("sp", None, None),
        P("sp", None, None),
        P("sp", None, None),
    )
    return jax.shard_map(
        body, mesh=mesh, in_specs=placed, out_specs=P(("sp", "tp"), None), check_vma=False
    )
```

profile of v0, /device:TPU:0, one launch (start us, length us, event | category | flops | bytes accessed | tf_op | source)
XLA Modules:
  0.0 186.5 jit_solution(3365401490658242660)
XLA Ops:
  7.3 0.8 slice.297
  8.0 1.7 collective-permute-start
  9.7 1.8 multiply_convert_fusion.2
  11.5 3.4 %collective-permute-start.1 = (bf16[30,128]{1,0:T(8,128)(2,1)S(1)}, bf16[30,128]{1,0:T(8,128)(2,1)S(1)}, u32[]{:S(2)}, u32[]{:S(2)}) collective-permute-start(bf16[30,128]{1,0:T(8,128)(2,1)S(1)} %slice.402), channel_id=1, source_target_pairs={{0,16},{16,32},{32,48},{48,64},{64,80},{80,96},{96,112},{112,128},... | collective-permute-start | bytes 23048 | tf_op jit(solution)/shard_map/ppermute | solution.py:12
  15.4 0.8 collective-permute-done.1
  16.3 16.6 %add_convert_fusion = bf16[3072,128]{1,0:T(8,128)(2,1)} fusion(bf16[3072,128]{1,0:T(8,128)(2,1)S(1)} %multiply_convert_fusion.2, bf16[30,128]{1,0:T(8,128)(2,1)S(1)} %collective-permute-done.1, f32[128]{0:T(128)S(1)} %get-tuple-element.14, f32[128]{0:T(128)S(1)} %get-tuple-element.15, f32[128]{0:T(128)S(1)} %get-tuple-element.16, ...), kind=kLoop, calls=%fused_computation.60 | loop fusion | flops 83755008 | bytes 1688576 | tf_op jit(solution)/shard_map/convert_element_type | solution.py:60
  32.9 8.7 %all-to-all-start = ((bf16[16,192,128]{2,1,0:T(8,128)(2,1)}), bf16[16,192,128]{2,1,0:T(8,128)(2,1)S(1)}, u32[]{:S(2)}, u32[]{:S(2)}) async-start(bf16[16,192,128]{2,1,0:T(8,128)(2,1)} %bitcast.147), calls=%async_computation | async-start | bytes 1572864 | tf_op jit(solution)/shard_map/all_to_all | solution.py:61
  42.0 0.9 reduce-window.6
  43.5 2.9 %scatter_custom_fusion = s32[384]{0:T(512)S(1)} fusion(s32[384]{0:T(512)S(1)} %fusion.132, s32[384]{0:T(512)S(1)} %add_select_fusion, s32[]{:T(128)} %constant.50.clone.1), kind=kCustom, calls=%fused_computation.261 | custom fusion | bytes 1540 | tf_op jit(solution)/shard_map/scatter | solution.py:112
  46.5 25.0 %all-to-all-done = bf16[16,192,128]{2,1,0:T(8,128)(2,1)S(1)} async-done(((bf16[16,192,128]{2,1,0:T(8,128)(2,1)}), bf16[16,192,128]{2,1,0:T(8,128)(2,1)S(1)}, u32[]{:S(2)}, u32[]{:S(2)}) %all-to-all-start) | async-done | bytes 786464 | tf_op jit(solution)/shard_map/all_to_all | solution.py:61
  72.1 11.1 %all-gather.2.cloned.1.call-done = bf16[2048,2048]{1,0:T(8,128)(2,1)} async-done(((bf16[128,2048]{1,0:T(8,128)(2,1)}), bf16[2048,2048]{1,0:T(8,128)(2,1)}) %all-gather.2.cloned.1.call-update) | async-done | bytes 8388624 | tf_op jit(solution)/shard_map/all_gather | solution.py:18
  83.2 5.7 %multiply_reduce_fusion = (f32[192]{0:T(256)S(1)}, f32[192,2048]{1,0:T(8,128)S(1)}) fusion(bf16[2048,2048]{1,0:T(8,128)(2,1)} %all-gather.2.cloned.1.call-done, f32[2048]{0:T(1024)S(1)} %copy-done.11, f32[2048]{0:T(1024)S(1)} %copy-done.12, f32[192]{0:T(256)S(1)} %add_rsqrt_fusion.1, f32[192]{0:T(256)S(1)} %broadcast_multiply_fusion.1, ...), kind=kOutput, calls=%fused_computation.58 | convolution fusion | flops 1616903936 | bytes 11553024 | tf_op jit(solution)/shard_map/dot_general | solution.py:16
  88.9 1.1 copy-done.1
  90.2 3.1 %gather_fusion = bf16[384,2048]{1,0:T(8,128)(2,1)} fusion(bf16[192,2048]{1,0:T(8,128)(2,1)S(1)} %multiply_convert_fusion, s32[1024]{0:T(1024)S(1)} %pad_clamp_fusion.1), kind=kCustom, calls=%fused_computation | custom fusion | bytes 3147264 | tf_op jit(solution)/shard_map/gather | solution.py:114
  93.3 30.1 %all_to_all.23 = bf16[16,24,2048]{2,1,0:T(8,128)(2,1)S(1)} all-to-all(bf16[16,24,2048]{2,1,0:T(8,128)(2,1)} %bitcast.146), channel_id=1, replica_groups=mesh['sp'=16,'tp'=16] {'sp'}, dimensions={0} | all-to-all | bytes 3145728 | tf_op jit(solution)/shard_map/all_to_all | solution.py:115
  123.5 1.2 copy-done.3
  124.6 1.9 fusion.5
  126.5 5.3 %convolution_convert_fusion = bf16[384,2048]{1,0:T(8,128)(2,1)} fusion(bf16[1,512,2048]{2,1,0:T(8,128)(2,1)S(1)} %copy-done, bf16[384,2048]{1,0:T(8,128)(2,1)} %bitcast.150, bf16[1,2048,512]{2,1,0:T(8,128)(2,1)} %param.28, f32[384,512]{1,0:T(8,128)} %fusion.5), kind=kOutput, calls=%fused_computation.32 | convolution fusion | flops 1612578816 | bytes 8126464 | tf_op jit(solution)/shard_map/dot_general | solution.py:121
  131.8 4.7 %all-to-all-start.2 = ((bf16[16,24,2048]{2,1,0:T(8,128)(2,1)}), bf16[16,24,2048]{2,1,0:T(8,128)(2,1)}, u32[]{:S(2)}, u32[]{:S(2)}) async-start(bf16[16,24,2048]{2,1,0:T(8,128)(2,1)} %bitcast.148), calls=%async_computation.2 | async-start | bytes 3145728 | tf_op jit(solution)/shard_map/all_to_all | solution.py:124
  137.3 22.2 %all-to-all-done.2 = bf16[16,24,2048]{2,1,0:T(8,128)(2,1)} async-done(((bf16[16,24,2048]{2,1,0:T(8,128)(2,1)}), bf16[16,24,2048]{2,1,0:T(8,128)(2,1)}, u32[]{:S(2)}, u32[]{:S(2)}) %all-to-all-start.2) | async-done | bytes 1572896 | tf_op jit(solution)/shard_map/all_to_all | solution.py:124
  159.5 6.7 %gather_fusion.1 = bf16[384,2048]{1,0:T(8,128)(2,1)} fusion(bf16[384,2048]{1,0:T(8,128)(2,1)} %bitcast.43, s32[1024]{0:T(1024)S(1)} %pad_clamp_fusion), kind=kCustom, calls=%fused_computation.1 | custom fusion | bytes 3147264 | tf_op jit(solution)/shard_map/gather | solution.py:132
  166.2 4.7 %reshape.154 = f32[192,2,2048]{2,1,0:T(2,128)} reshape(bf16[384,2048]{1,0:T(8,128)(2,1)} %gather_fusion.1) | data formatting | bytes 4718592 | tf_op jit(solution)/shard_map/convert_element_type | solution.py:134
  170.9 6.2 %fusion.138 = (f32[192,1,2048]{2,1,0:T(1,128)S(1)}, f32[192,1,2048]{2,1,0:T(1,128)S(1)}) fusion(f32[192,2,2048]{2,1,0:T(2,128)} %reshape.154), kind=kLoop, calls=%fused_computation.302 | loop fusion | bytes 6291456 | tf_op jit(solution)/shard_map/slice | solution.py:136
  177.1 2.6 %fusion.15 = bf16[192,2048]{1,0:T(8,128)(2,1)} fusion(f32[192,2048]{1,0:T(8,128)S(1)} %copy-done.2, f32[192,1,2048]{2,1,0:T(1,128)S(1)} %get-tuple-element.12, f32[192,1,2048]{2,1,0:T(1,128)S(1)} %get-tuple-element.11, f32[192]{0:T(256)S(1)} %multiply_divide_fusion, f32[192]{0:T(256)S(1)} %get-tuple-element.9), kind=kLoop, calls=%fused_computation.54 | loop fusion | flops 1966080 | bytes 5506560 | tf_op jit(solution)/shard_map/convert_element_type | solution.py:137
  (61 shorter events, 3.8 us)
Async XLA Ops:
  6.5 119.9 %copy-start = (bf16[1,512,2048]{2,1,0:T(8,128)(2,1)S(1)}, bf16[1,512,2048]{2,1,0:T(8,128)(2,1)}, u32[]{:S(2)}) copy-start(bf16[1,512,2048]{2,1,0:T(8,128)(2,1)} %param.29) | copy-start | bytes 6291460
  6.5 8.5 %copy-start.4 = (s32[3072]{0:T(1024)S(1)}, s32[3072]{0:T(1024)}, u32[]{:S(2)}) copy-start(s32[3072]{0:T(1024)} %param.17) | copy-start | bytes 36868
  6.5 8.4 %copy-start.9 = (bf16[31,128]{1,0:T(8,128)(2,1)S(1)}, bf16[31,128]{1,0:T(8,128)(2,1)}, u32[]{:S(2)}) copy-start(bf16[31,128]{1,0:T(8,128)(2,1)} %param.18) | copy-start | bytes 23812
  6.5 76.6 %all-gather.2.cloned.1.call-start = ((), (), s32[]{:S(2)}) async-start(), calls=%async_computation.3 | async-start | bytes 8912896 | tf_op jit(solution)/shard_map/all_gather | solution.py:18
  8.0 7.0 %collective-permute-start = (s32[30]{0:T(128)S(1)}, s32[30]{0:T(128)S(1)}, u32[]{:S(2)}, u32[]{:S(2)}) collective-permute-start(s32[30]{0:T(128)S(1)} %slice.297), channel_id=1, source_target_pairs={{0,16},{16,32},{32,48},{48,64},{64,80},{80,96},{96,112},{112,128},... | collective-permute-start | bytes 368 | tf_op jit(solution)/shard_map/ppermute | solution.py:12
  11.5 4.8 %collective-permute-start.1 = (bf16[30,128]{1,0:T(8,128)(2,1)S(1)}, bf16[30,128]{1,0:T(8,128)(2,1)S(1)}, u32[]{:S(2)}, u32[]{:S(2)}) collective-permute-start(bf16[30,128]{1,0:T(8,128)(2,1)S(1)} %slice.402), channel_id=1, source_target_pairs={{0,16},{16,32},{32,48},{48,64},{64,80},{80,96},{96,112},{112,128},... | collective-permute-start | bytes 23048 | tf_op jit(solution)/shard_map/ppermute | solution.py:12
  16.3 25.3 %copy-start.6 = (s32[192,2]{0,1:T(2,128)S(1)}, s32[192,2]{0,1:T(2,128)}, u32[]{:S(2)}) copy-start(s32[192,2]{0,1:T(2,128)} %param.26) | copy-start | bytes 4612
  32.9 50.3 %copy-start.11 = (f32[2048]{0:T(1024)S(1)}, f32[2048]{0:T(1024)}, u32[]{:S(2)}) copy-start(f32[2048]{0:T(1024)} %param.20) | copy-start | bytes 24580
  32.9 50.3 %copy-start.12 = (f32[2048]{0:T(1024)S(1)}, f32[2048]{0:T(1024)}, u32[]{:S(2)}) copy-start(f32[2048]{0:T(1024)} %param.19) | copy-start | bytes 24580
  32.9 38.6 %all-to-all-start = ((bf16[16,192,128]{2,1,0:T(8,128)(2,1)}), bf16[16,192,128]{2,1,0:T(8,128)(2,1)S(1)}, u32[]{:S(2)}, u32[]{:S(2)}) async-start(bf16[16,192,128]{2,1,0:T(8,128)(2,1)} %bitcast.147), calls=%async_computation | async-start | bytes 1572864 | tf_op jit(solution)/shard_map/all_to_all | solution.py:61
  72.1 18.0 %copy-start.7 = (f32[2048]{0:T(1024)S(1)}, f32[2048]{0:T(1024)}, u32[]{:S(2)}) copy-start(f32[2048]{0:T(1024)} %param.23) | copy-start | bytes 24580
  88.9 1.1 copy-start.1
  93.3 31.3 %copy-start.10 = (bf16[1,2048,512]{2,1,0:T(8,128)(2,1)S(1)}, bf16[1,2048,512]{2,1,0:T(8,128)(2,1)}, u32[]{:S(2)}) copy-start(bf16[1,2048,512]{2,1,0:T(8,128)(2,1)} %param.27) | copy-start | bytes 6291460
  123.5 1.2 copy-start.3
  131.8 4.7 %copy-start.8 = (bf16[2048,2]{0,1:T(2,128)(2,1)S(1)}, bf16[2048,2]{0,1:T(2,128)(2,1)}, u32[]{:S(2)}) copy-start(bf16[2048,2]{0,1:T(2,128)(2,1)} %param.24) | copy-start | bytes 24580
  131.8 5.1 %copy-start.5 = (bf16[2048,16]{0,1:T(8,128)(2,1)S(1)}, bf16[2048,16]{0,1:T(8,128)(2,1)}, u32[]{:S(2)}) copy-start(bf16[2048,16]{0,1:T(8,128)(2,1)} %param.25) | copy-start | bytes 196612
  131.8 27.7 %all-to-all-start.2 = ((bf16[16,24,2048]{2,1,0:T(8,128)(2,1)}), bf16[16,24,2048]{2,1,0:T(8,128)(2,1)}, u32[]{:S(2)}, u32[]{:S(2)}) async-start(bf16[16,24,2048]{2,1,0:T(8,128)(2,1)} %bitcast.148), calls=%async_computation.2 | async-start | bytes 3145728 | tf_op jit(solution)/shard_map/all_to_all | solution.py:124
  170.9 6.2 %copy-start.2 = (f32[192,2048]{1,0:T(8,128)S(1)}, f32[192,2048]{1,0:T(8,128)}, u32[]{:S(2)}) copy-start(f32[192,2048]{1,0:T(8,128)} %copy-done.1) | copy-start | bytes 4718596
Sparse Core Ops, SparseCore 0:
  9.2 73.9 all-gather.1
where the time goes:
time: 187 us
  waiting for transfers between devices  59.9 us (32%)
  blocking collectives  30.1 us (16%)
  local copies, waits for them, and re-layouts  27.6 us (15%)
  other arithmetic  23.2 us (12%)
  starting transfers between devices  18.5 us (10%)
  between operations  13.7 us (7%)
  matrix products  13.5 us (7%)
    all_to_all x1, blocking collectives, body(): lax.all_to_all(outgoing, 'sp', split_axis=0, concat_axis=0, tiled=True)  30.1 us
    all_to_all x1, waiting for transfers between devices, body(): lax.all_to_all(convolved, 'tp', split_axis=0, concat_axis=1, tiled=True)  25 us
    all_to_all x1, waiting for transfers between devices, body(): lax.all_to_all(expert_result.reshape(senders, slot_count, features), 'sp'...  22.2 us
    convert_element_type x1, other arithmetic, body(): convolved = summed.astype(jnp.bfloat16)  16.6 us
    all_gather x1, waiting for transfers between devices, project_rows(): lax.all_gather(proj_weight, 'tp', axis=0, tiled=True)  11.1 us
    all_to_all x1, starting transfers between devices, body(): lax.all_to_all(convolved, 'tp', split_axis=0, concat_axis=1, tiled=True)  8.7 us
    gather x1, local copies, waits for them, and re-layouts, body(): returned.reshape(2 * row_count, normed.shape[1])[destination]  6.68 us
    slice x1, local copies, waits for them, and re-layouts, body(): picked[:, 0]  6.18 us
  transfers between devices with their start and end apart: 5, of which 4 were waited for; matrix products, arithmetic and copies ran while one was open for 14% of the time, Pallas kernels for 0%

commit v1 on v0

--- a/solution.py
+++ b/solution.py
@@ -15,7 +15,9 @@
 def project_rows(activated_rows, proj_weight):
     return jnp.dot(
         activated_rows,
-        lax.all_gather(proj_weight, "tp", axis=0, tiled=True),
+        jnp.concatenate(
+            lax.all_to_all(jnp.stack([proj_weight] * lax.axis_size("tp")), "tp", 0, 0), axis=0
+        ),
         preferred_element_type=jnp.float32,
     )
 

time: 187 us -> 347 us (1.86)
  waiting for transfers between devices: 59.9 us -> 201 us
  blocking collectives: 30.1 us -> 60.9 us
  between operations: 13.7 us -> 0.34 us
  starting transfers between devices: 18.5 us -> 14.5 us
  local copies, waits for them, and re-layouts: 27.6 us -> 31.2 us
    all_to_all x1, waiting for transfers between devices: 25 us -> 179 us  [project_rows(): lax.all_to_all(jnp.stack([proj_weight] * lax.axis_size('tp')), 'tp', 0, 0)]
    all_to_all x0 -> x1, blocking collectives: none -> 30.7 us  [body(): lax.all_to_all(convolved, 'tp', split_axis=0, concat_axis=1, tiled=True)]
    all_gather x1 -> x0, waiting for transfers between devices: 11.1 us -> none  [project_rows(): lax.all_gather(proj_weight, 'tp', axis=0, tiled=True)]
    another operation x0 -> x1, local copies, waits for them, and re-layouts: none -> 4.28 us  [project_rows(): jnp.stack([proj_weight] * lax.axis_size('tp'))]
    all_to_all x1, starting transfers between devices: 8.7 us -> 4.87 us  [project_rows(): lax.all_to_all(jnp.stack([proj_weight] * lax.axis_size('tp')), 'tp', 0, 0)]
  transfers between devices with their start and end apart: 5 -> 4, of which waited for: 4 -> 3; matrix products, arithmetic and copies ran while one was open for 14% -> 2% of each run, Pallas kernels for 0% -> 0%
where the time goes in v1:
time: 347 us; the launch traced here: 345 us
  waiting for transfers between devices  201 us (58%)
  blocking collectives  60.9 us (18%)
  local copies, waits for them, and re-layouts  31.2 us (9%)
  other arithmetic  22.6 us (7%)
  starting transfers between devices  14.5 us (4%)
  matrix products  13.5 us (4%)
    all_to_all x1, waiting for transfers between devices, project_rows(): lax.all_to_all(jnp.stack([proj_weight] * lax.axis_size('tp')), 'tp', 0, 0)  179 us
    all_to_all x1, blocking collectives, body(): lax.all_to_all(convolved, 'tp', split_axis=0, concat_axis=1, tiled=True)  30.7 us
    all_to_all x1, blocking collectives, body(): lax.all_to_all(outgoing, 'sp', split_axis=0, concat_axis=0, tiled=True)  30.1 us
    all_to_all x1, waiting for transfers between devices, body(): lax.all_to_all(expert_result.reshape(senders, slot_count, features), 'sp'...  21.7 us
    convert_element_type x1, other arithmetic, body(): convolved = summed.astype(jnp.bfloat16)  15.9 us
  transfers between devices with their start and end apart: 4, of which 3 were waited for; matrix products, arithmetic and copies ran while one was open for 2% of the time, Pallas kernels for 0%

profile of v1, /device:TPU:0, one launch (start us, length us, event | category | flops | bytes accessed | tf_op | source)
XLA Modules:
  0.0 344.5 jit_solution(3846514867258101514)
XLA Ops:
  0.0 1.9 multiply_convert_fusion.1
  2.0 1.7 collective-permute-start.1
  3.7 3.4 collective-permute-start
  7.2 1.2 collective-permute-done
  8.9 15.9 %add_convert_fusion = bf16[3072,128]{1,0:T(8,128)(2,1)S(1)} fusion(bf16[3072,128]{1,0:T(8,128)(2,1)S(1)} %multiply_convert_fusion.1, bf16[30,128]{1,0:T(8,128)(2,1)S(1)} %collective-permute-done.1, f32[128]{0:T(128)S(1)} %get-tuple-element.14, f32[128]{0:T(128)S(1)} %get-tuple-element.15, f32[128]{0:T(128)S(1)} %get-tuple-element.16, ...), kind=kLoop, calls=%fused_computation.65 | loop fusion | flops 83755008 | bytes 1688576 | tf_op jit(solution)/shard_map/convert_element_type | solution.py:62
  24.8 30.7 %all_to_all.28 = bf16[16,192,128]{2,1,0:T(8,128)(2,1)S(1)} all-to-all(bf16[16,192,128]{2,1,0:T(8,128)(2,1)S(1)} %bitcast.158), channel_id=1, replica_groups=mesh['sp'=16,'tp'=16] {'tp'}, dimensions={0} | all-to-all | bytes 1572864 | tf_op jit(solution)/shard_map/all_to_all | solution.py:63
  55.5 4.3 %stack.2 = bf16[16,128,2048]{2,1,0:T(8,128)(2,1)} broadcast(bf16[128,2048]{1,0:T(8,128)(2,1)S(1)} %copy-done.4), dimensions={1,2} | broadcast | bytes 8912896 | tf_op jit(solution)/shard_map/stack | solution.py:19
  59.8 4.9 %all-to-all-start.1 = ((bf16[16,128,2048]{2,1,0:T(8,128)(2,1)}), bf16[16,128,2048]{2,1,0:T(8,128)(2,1)}, u32[]{:S(2)}, u32[]{:S(2)}) async-start(bf16[16,128,2048]{2,1,0:T(8,128)(2,1)} %stack.2), calls=%async_computation.1 | async-start | bytes 16777216 | tf_op jit(solution)/shard_map/all_to_all | solution.py:19
  65.4 0.9 reduce-window.6
  66.6 2.9 scatter_custom_fusion
  70.1 178.6 %all-to-all-done.1 = bf16[16,128,2048]{2,1,0:T(8,128)(2,1)} async-done(((bf16[16,128,2048]{2,1,0:T(8,128)(2,1)}), bf16[16,128,2048]{2,1,0:T(8,128)(2,1)}, u32[]{:S(2)}, u32[]{:S(2)}) %all-to-all-start.1) | async-done | bytes 8388640 | tf_op jit(solution)/shard_map/all_to_all | solution.py:19
  248.7 5.7 %multiply_reduce_fusion = (f32[192]{0:T(256)S(1)}, f32[192,2048]{1,0:T(8,128)S(1)}) fusion(bf16[16,128,2048]{2,1,0:T(8,128)(2,1)} %all-to-all-done.1, bf16[16,192,128]{2,1,0:T(8,128)(2,1)S(1)} %all_to_all.28, f32[16,128]{1,0:T(8,128)S(1)} %bitcast.166, f32[16,128]{1,0:T(8,128)S(1)} %bitcast.167, f32[192]{0:T(256)S(1)} %add_rsqrt_fusion.1, ...), kind=kOutput, calls=%fused_computation.64 | convolution fusion | flops 1616903936 | bytes 11553024 | tf_op jit(solution)/shard_map/dot_general | solution.py:16
  254.5 1.1 copy-done.1
  255.8 3.1 gather_fusion
  258.9 30.1 %all_to_all.29 = bf16[16,24,2048]{2,1,0:T(8,128)(2,1)S(1)} all-to-all(bf16[16,24,2048]{2,1,0:T(8,128)(2,1)} %bitcast.157), channel_id=1, replica_groups=mesh['sp'=16,'tp'=16] {'sp'}, dimensions={0} | all-to-all | bytes 3145728 | tf_op jit(solution)/shard_map/all_to_all | solution.py:117
  289.1 1.2 copy-done.3
  290.2 1.9 fusion.6
  292.1 5.3 %convolution_convert_fusion = bf16[384,2048]{1,0:T(8,128)(2,1)} fusion(bf16[1,512,2048]{2,1,0:T(8,128)(2,1)S(1)} %copy-done, bf16[384,2048]{1,0:T(8,128)(2,1)} %bitcast.161, bf16[1,2048,512]{2,1,0:T(8,128)(2,1)} %param.28, f32[384,512]{1,0:T(8,128)} %fusion.6), kind=kOutput, calls=%fused_computation.32 | convolution fusion | flops 1612578816 | bytes 8126464 | tf_op jit(solution)/shard_map/dot_general | solution.py:123
  297.4 4.5 %all-to-all-start.3 = ((bf16[16,24,2048]{2,1,0:T(8,128)(2,1)}), bf16[16,24,2048]{2,1,0:T(8,128)(2,1)}, u32[]{:S(2)}, u32[]{:S(2)}) async-start(bf16[16,24,2048]{2,1,0:T(8,128)(2,1)} %bitcast.159), calls=%async_computation.3 | async-start | bytes 3145728 | tf_op jit(solution)/shard_map/all_to_all | solution.py:126
  302.7 21.7 %all-to-all-done.3 = bf16[16,24,2048]{2,1,0:T(8,128)(2,1)} async-done(((bf16[16,24,2048]{2,1,0:T(8,128)(2,1)}), bf16[16,24,2048]{2,1,0:T(8,128)(2,1)}, u32[]{:S(2)}, u32[]{:S(2)}) %all-to-all-start.3) | async-done | bytes 1572896 | tf_op jit(solution)/shard_map/all_to_all | solution.py:126
  324.4 6.7 %gather_fusion.1 = bf16[384,2048]{1,0:T(8,128)(2,1)} fusion(bf16[384,2048]{1,0:T(8,128)(2,1)} %bitcast.46, s32[1024]{0:T(1024)S(1)} %pad_clamp_fusion), kind=kCustom, calls=%fused_computation.1 | custom fusion | bytes 3147264 | tf_op jit(solution)/shard_map/gather | solution.py:134
  331.1 4.7 %reshape.175 = f32[192,2,2048]{2,1,0:T(2,128)} reshape(bf16[384,2048]{1,0:T(8,128)(2,1)} %gather_fusion.1) | data formatting | bytes 4718592 | tf_op jit(solution)/shard_map/convert_element_type | solution.py:136
  335.8 6.2 %fusion.147 = (f32[192,1,2048]{2,1,0:T(1,128)S(1)}, f32[192,1,2048]{2,1,0:T(1,128)S(1)}) fusion(f32[192,2,2048]{2,1,0:T(2,128)} %reshape.175), kind=kLoop, calls=%fused_computation.307 | loop fusion | bytes 6291456 | tf_op jit(solution)/shard_map/slice | solution.py:138
  342.0 2.6 fusion.23
  (62 shorter events, 3.1 us)
Async XLA Ops:
  0.0 292.1 %copy-start = (bf16[1,512,2048]{2,1,0:T(8,128)(2,1)S(1)}, bf16[1,512,2048]{2,1,0:T(8,128)(2,1)}, u32[]{:S(2)}) copy-start(bf16[1,512,2048]{2,1,0:T(8,128)(2,1)} %param.29) | copy-start | bytes 6291460
  0.0 3.7 %copy-start.5 = (s32[3072]{0:T(1024)S(1)}, s32[3072]{0:T(1024)}, u32[]{:S(2)}) copy-start(s32[3072]{0:T(1024)} %param.17) | copy-start | bytes 36868
  0.0 7.1 %copy-start.10 = (bf16[31,128]{1,0:T(8,128)(2,1)S(1)}, bf16[31,128]{1,0:T(8,128)(2,1)}, u32[]{:S(2)}) copy-start(bf16[31,128]{1,0:T(8,128)(2,1)} %param.18) | copy-start | bytes 23812
  2.0 6.9 %collective-permute-start.1 = (bf16[30,128]{1,0:T(8,128)(2,1)S(1)}, bf16[30,128]{1,0:T(8,128)(2,1)S(1)}, u32[]{:S(2)}, u32[]{:S(2)}) collective-permute-start(bf16[30,128]{1,0:T(8,128)(2,1)S(1)} %slice.402), channel_id=1, source_target_pairs={{0,16},{16,32},{32,48},{48,64},{64,80},{80,96},{96,112},{112,128},... | collective-permute-start | bytes 23048 | tf_op jit(solution)/shard_map/ppermute | solution.py:12
  3.7 4.7 %collective-permute-start = (s32[30]{0:T(128)S(1)}, s32[30]{0:T(128)S(1)}, u32[]{:S(2)}, u32[]{:S(2)}) collective-permute-start(s32[30]{0:T(128)S(1)} %slice.297), channel_id=1, source_target_pairs={{0,16},{16,32},{32,48},{48,64},{64,80},{80,96},{96,112},{112,128},... | collective-permute-start | bytes 368 | tf_op jit(solution)/shard_map/ppermute | solution.py:12
  8.9 46.6 %copy-start.4 = (bf16[128,2048]{1,0:T(8,128)(2,1)S(1)}, bf16[128,2048]{1,0:T(8,128)(2,1)}, u32[]{:S(2)}) copy-start(bf16[128,2048]{1,0:T(8,128)(2,1)} %param.21) | copy-start | bytes 1572868
  59.8 4.9 %copy-start.7 = (s32[192,2]{0,1:T(2,128)S(1)}, s32[192,2]{0,1:T(2,128)}, u32[]{:S(2)}) copy-start(s32[192,2]{0,1:T(2,128)} %param.26) | copy-start | bytes 4612
  59.8 189.0 %all-to-all-start.1 = ((bf16[16,128,2048]{2,1,0:T(8,128)(2,1)}), bf16[16,128,2048]{2,1,0:T(8,128)(2,1)}, u32[]{:S(2)}, u32[]{:S(2)}) async-start(bf16[16,128,2048]{2,1,0:T(8,128)(2,1)} %stack.2), calls=%async_computation.1 | async-start | bytes 16777216 | tf_op jit(solution)/shard_map/all_to_all | solution.py:19
  64.7 184.1 %copy-start.12 = (f32[2048]{0:T(1024)S(1)}, f32[2048]{0:T(1024)}, u32[]{:S(2)}) copy-start(f32[2048]{0:T(1024)} %param.20) | copy-start | bytes 24580
  64.7 184.1 %copy-start.13 = (f32[2048]{0:T(1024)S(1)}, f32[2048]{0:T(1024)}, u32[]{:S(2)}) copy-start(f32[2048]{0:T(1024)} %param.19) | copy-start | bytes 24580
  248.7 6.9 %copy-start.8 = (f32[2048]{0:T(1024)S(1)}, f32[2048]{0:T(1024)}, u32[]{:S(2)}) copy-start(f32[2048]{0:T(1024)} %param.23) | copy-start | bytes 24580
  254.5 1.1 copy-start.1
  258.9 31.3 %copy-start.11 = (bf16[1,2048,512]{2,1,0:T(8,128)(2,1)S(1)}, bf16[1,2048,512]{2,1,0:T(8,128)(2,1)}, u32[]{:S(2)}) copy-start(bf16[1,2048,512]{2,1,0:T(8,128)(2,1)} %param.27) | copy-start | bytes 6291460
  289.1 1.2 copy-start.3
  297.4 4.6 %copy-start.9 = (bf16[2048,2]{0,1:T(2,128)(2,1)S(1)}, bf16[2048,2]{0,1:T(2,128)(2,1)}, u32[]{:S(2)}) copy-start(bf16[2048,2]{0,1:T(2,128)(2,1)} %param.24) | copy-start | bytes 24580
  297.4 4.9 %copy-start.6 = (bf16[2048,16]{0,1:T(8,128)(2,1)S(1)}, bf16[2048,16]{0,1:T(8,128)(2,1)}, u32[]{:S(2)}) copy-start(bf16[2048,16]{0,1:T(8,128)(2,1)} %param.25) | copy-start | bytes 196612
  297.4 27.0 %all-to-all-start.3 = ((bf16[16,24,2048]{2,1,0:T(8,128)(2,1)}), bf16[16,24,2048]{2,1,0:T(8,128)(2,1)}, u32[]{:S(2)}, u32[]{:S(2)}) async-start(bf16[16,24,2048]{2,1,0:T(8,128)(2,1)} %bitcast.159), calls=%async_computation.3 | async-start | bytes 3145728 | tf_op jit(solution)/shard_map/all_to_all | solution.py:126
  335.8 6.2 %copy-start.2 = (f32[192,2048]{1,0:T(8,128)S(1)}, f32[192,2048]{1,0:T(8,128)}, u32[]{:S(2)}) copy-start(f32[192,2048]{1,0:T(8,128)} %copy-done.1) | copy-start | bytes 4718596
